TPU v7x, 32 devices: a whole 2x2x4 slice. The times are simulated.
32 devices in a mesh: dp: 4 (over y, x), kv: 4 (over z), tp: 2 (over core).
Axes of the slice: x: 2, y: 2, z: 4, core: 2. Of those that a mesh axis runs over, the one named last changes fastest.
Arguments:
- piece_tokens: bfloat16 [2048, 2048], P(('dp', 'kv')), parts along dimension 0, may hold values from -6 to 6
- step_tokens: bfloat16 [16, 2048], P(('dp', 'kv')), parts along dimension 0, may hold values from -6 to 6
- norm_gain: float32 [2048], replicated, may hold values from 0.1 to 1.9
- query_weight: bfloat16 [2048, 1024], P(None, 'tp'), may hold values from -0.125 to 0.125
- key_weight: bfloat16 [2048, 1024], P(None, 'tp'), may hold values from -0.125 to 0.125
- value_weight: bfloat16 [2048, 1024], P(None, 'tp'), may hold values from -0.125 to 0.125
- gate_weight: bfloat16 [2048, 16], replicated, may hold values from -0.125 to 0.125
- gate_bias: float32 [16], replicated, may hold values from 3 to 10.5
- out_weight: bfloat16 [1024, 2048], P(None, 'tp'), may hold values from -0.1875 to 0.1875
- cache_keys: bfloat16 [8192, 1024], P(('dp', 'kv'), 'tp'), parts along dimension 0, may hold values from -320 to 320
- cache_values: bfloat16 [8192, 1024], P(('dp', 'kv'), 'tp'), parts along dimension 0, may hold values from -10 to 10
- cache_decay: float32 [16, 8192], P('tp', ('dp', 'kv')), parts along dimension 1, may hold values from -696.32 to 0, as said below
- decay_total: float32 [64], P('dp'), parts along dimension 0, may hold values from -696.32 to 0, as said below
- step_keys: bfloat16 [16, 1024, 1024], P(('dp', 'kv'), None, 'tp'), parts along dimension 0, may hold values from -6 to 6
- step_values: bfloat16 [16, 1024, 1024], P(('dp', 'kv'), None, 'tp'), parts along dimension 0, may hold values from -6 to 6
- step_gates: float32 [16, 16, 1024], P(('dp', 'kv'), 'tp'), parts along dimension 0, may hold values from -0.34 to 0
- step_lengths: int32 [16], P(('dp', 'kv')), parts along dimension 0, may hold values from 1 to 1024, 2048 in all
Outputs:
- piece_out: bfloat16 [2048, 2048], P(('dp', 'kv'), 'tp'), parts along dimension 0
- step_out: bfloat16 [16, 2048], P(('dp', 'kv'), 'tp'), parts along dimension 0
There are 4 independent parts, one for each index of `dp`. A program takes and returns all parts, laid end to end along the dimension named above; an argument that names none is the same for every part. Nothing has to cross between parts.
Inputs may be any that keep to these rules, and one draw needn't show every extreme that they name: `cache_decay`: cumulative values never rise along the positions and start at one gate below zero. `decay_total`: equal to the cumulative value of the last cached position. `step_lengths`: each length is 1 to 1024; the largest is exactly 1024; positions at or past a length are unused.
All inputs are finite; a program needn't handle non-finite values.
Results may differ from a plain program's by a relative error of at most 0.0095.
The roundings to bfloat16 on the way count: a program that leaves them out, or rounds other values in their place, can miss the bound.
Values may be sent and summed in bfloat16 or wider, within the bound.
A program may use at most 128 MiB of HBM per device.

v0:
```python
import jax
import jax.numpy as jnp
from jax import lax
from jax.sharding import PartitionSpec as P

norm_eps = 1e-06
negative = -1e30


def carried_in(value, axis, join, neutral):
    count, mine = (lax.axis_size(axis), lax.axis_index(axis))
    pieces = lax.all_gather(value, axis)
    total = jnp.full_like(value, 0) + jnp.asarray(neutral, value.dtype)

    def step(position, total):
        longer = join(total, pieces[position])
        return jnp.where(position < mine, longer, total)

    return lax.fori_loop(0, count - 1, step, total)


def normalize(token_rows, norm_gain):
    wide = token_rows.astype(jnp.float32)
    factor = lax.rsqrt(jnp.mean(wide * wide, axis=-1, keepdims=True) + norm_eps)
    return (wide * factor * norm_gain).astype(jnp.bfloat16)


def attend_piece(queries, positions, all_keys, all_values, key_bias, key_slots, cache_len):
    head_count = key_bias.shape[0]
    query_count = queries.shape[0]
    head_width = all_keys.shape[1] // head_count
    score_scale = head_width ** (-0.5)
    key_heads = all_keys.reshape(all_keys.shape[0], head_count, head_width)
    value_heads = all_values.reshape(all_values.shape[0], head_count, head_width)

    def one_block(block_args):
        block_q, block_pos = block_args
        row_count = block_q.shape[0]
        scores = (
            jnp.einsum(
                "qhd,khd->hqk",
                block_q.reshape(row_count, head_count, head_width),
                key_heads,
                preferred_element_type=jnp.float32,
            )
            * score_scale
        )
        scores = scores + key_bias[:, None, :]
        visible = jnp.concatenate(
            [jnp.ones((row_count, cache_len), jnp.bool_), block_pos[:, None] >= key_slots[None, :]],
            axis=1,
        )
        scores = jnp.where(visible[None], scores, negative)
        row_high = jnp.max(scores, axis=-1)
        exp_scores = jnp.exp(scores - row_high[..., None])
        row_mass = jnp.sum(exp_scores, axis=-1)
        summed = jnp.einsum(
            "hqk,khd->qhd",
            exp_scores.astype(jnp.bfloat16),
            value_heads,
            preferred_element_type=jnp.float32,
        )
        part_means = (
            (summed / row_mass.T[:, :, None])
            .astype(jnp.bfloat16)
            .reshape(row_count, head_count * head_width)
        )
        return (part_means, row_high.T, row_mass.T)

    if query_count > 512 and query_count % 512 == 0:
        group_count = query_count // 512
        part_means, part_high, part_mass = lax.map(
            one_block, (queries.reshape(group_count, 512, -1), positions.reshape(group_count, 512))
        )
        return (
            part_means.reshape(query_count, -1),
            part_high.reshape(query_count, head_count),
            part_mass.reshape(query_count, head_count),
        )
    return one_block((queries, positions))


def combine(part_means, part_high, part_mass):
    best_high = jnp.max(part_high, axis=0)
    share = part_mass * jnp.exp(part_high - best_high[None])
    peer_count, row_count, head_count = share.shape
    part_float = part_means.reshape(peer_count, row_count, head_count, -1).astype(jnp.float32)
    summed = jnp.sum(share[..., None] * part_float, axis=0) / jnp.sum(share, axis=0)[..., None]
    return summed.astype(jnp.bfloat16).reshape(row_count, -1)


def per_device(
    piece_tokens,
    step_tokens,
    norm_gain,
    query_weight,
    key_weight,
    value_weight,
    gate_weight,
    gate_bias,
    out_weight,
    cache_keys,
    cache_values,
    cache_decay,
    decay_total,
    step_keys,
    step_values,
    step_gates,
    step_lengths,
):
    piece_rows = piece_tokens.shape[0]
    step_count = step_tokens.shape[0]
    head_count = cache_decay.shape[0]
    head_width = query_weight.shape[1] // head_count
    score_scale = head_width ** (-0.5)
    head_start = lax.axis_index("tp") * head_count
    token_rows = jnp.concatenate([piece_tokens, step_tokens], axis=0)
    normed = normalize(token_rows, norm_gain)
    queries = jnp.dot(normed, query_weight, preferred_element_type=jnp.float32).astype(jnp.bfloat16)
    new_keys = jnp.dot(normed, key_weight, preferred_element_type=jnp.float32).astype(jnp.bfloat16)
    new_values = jnp.dot(normed, value_weight, preferred_element_type=jnp.float32).astype(
        jnp.bfloat16
    )
    gate_cols = lax.dynamic_slice_in_dim(gate_weight, head_start, head_count, 1)
    bias_cols = lax.dynamic_slice_in_dim(gate_bias, head_start, head_count, 0)
    start_decay = lax.dynamic_slice_in_dim(decay_total, head_start, head_count, 0)
    log_gates = jax.nn.log_sigmoid(
        jnp.dot(normed, gate_cols, preferred_element_type=jnp.float32) + bias_cols
    )
    piece_gates = log_gates[:piece_rows]
    gate_before = carried_in(
        jnp.sum(piece_gates, axis=0), "kv", jnp.add, jnp.zeros((head_count,), jnp.float32)
    )
    piece_decay = start_decay + gate_before + jnp.cumsum(piece_gates, axis=0)
    key_bias = -jnp.concatenate([cache_decay, piece_decay.T], axis=1)
    all_keys = jnp.concatenate([cache_keys, new_keys[:piece_rows]], axis=0)
    all_values = jnp.concatenate([cache_values, new_values[:piece_rows]], axis=0)
    key_slots = lax.axis_index("kv") * piece_rows + jnp.arange(piece_rows, dtype=jnp.int32)
    cache_len = cache_keys.shape[0]
    peer_count = lax.axis_size("kv")
    own_queries = queries[:piece_rows]
    gathered = lax.all_gather(own_queries, "kv", axis=0, tiled=True)
    positions = jnp.arange(peer_count * piece_rows, dtype=jnp.int32)
    part_means, part_high, part_mass = attend_piece(
        gathered, positions, all_keys, all_values, key_bias, key_slots, cache_len
    )
    part_means = lax.all_to_all(part_means[None], "kv", split_axis=1, concat_axis=0, tiled=True)
    part_high, part_mass = (
        lax.all_to_all(part_high[None], "kv", split_axis=1, concat_axis=0, tiled=True),
        lax.all_to_all(part_mass[None], "kv", split_axis=1, concat_axis=0, tiled=True),
    )
    piece_att = combine(part_means, part_high, part_mass)
    cache_span = step_keys.shape[1]
    step_q = queries[piece_rows:].reshape(step_count, head_count, head_width)
    step_k = new_keys[piece_rows:].reshape(step_count, head_count, head_width)
    step_v = new_values[piece_rows:].reshape(step_count, head_count, head_width)
    step_lg = log_gates[piece_rows:]
    in_cache = jnp.arange(cache_span, dtype=jnp.int32)[None, :] < step_lengths[:, None]
    kept_gates = jnp.where(in_cache[:, None, :], step_gates, 0.0)
    running = jnp.cumsum(kept_gates, axis=2)
    after_sum = running[:, :, -1:] - running
    cache_scores = (
        jnp.einsum(
            "bhd,blhd->bhl",
            step_q,
            step_keys.reshape(step_count, cache_span, head_count, head_width),
            preferred_element_type=jnp.float32,
        )
        * score_scale
    )
    cache_scores = cache_scores + step_lg[:, :, None] + after_sum
    cache_scores = jnp.where(in_cache[:, None, :], cache_scores, negative)
    self_scores = (
        jnp.einsum("bhd,bhd->bh", step_q, step_k, preferred_element_type=jnp.float32) * score_scale
    )
    step_high = jnp.maximum(jnp.max(cache_scores, axis=-1), self_scores)
    cache_exp = jnp.exp(cache_scores - step_high[..., None])
    self_exp = jnp.exp(self_scores - step_high)
    step_mass = jnp.sum(cache_exp, axis=-1) + self_exp
    step_mix = jnp.einsum(
        "bhl,blhd->bhd",
        cache_exp.astype(jnp.bfloat16),
        step_values.reshape(step_count, cache_span, head_count, head_width),
        preferred_element_type=jnp.float32,
    )
    step_mix = step_mix + self_exp.astype(jnp.bfloat16).astype(jnp.float32)[
        ..., None
    ] * step_v.astype(jnp.float32)
    step_att = (
        (step_mix / step_mass[..., None])
        .astype(jnp.bfloat16)
        .reshape(step_count, head_count * head_width)
    )
    att_rows = jnp.concatenate([piece_att, step_att], axis=0)
    projected = jnp.dot(
        lax.all_gather(att_rows, "tp", axis=1, tiled=True),
        out_weight,
        preferred_element_type=jnp.float32,
    )
    projected = projected.astype(jnp.bfloat16)
    return (projected[:piece_rows], projected[piece_rows:])


def solution(mesh):
    in_specs = (
        P(("dp", "kv"), None),
        P(("dp", "kv"), None),
        P(),
        P(None, "tp"),
        P(None, "tp"),
        P(None, "tp"),
        P(),
        P(),
        P(None, "tp"),
        P(("dp", "kv"), "tp"),
        P(("dp", "kv"), "tp"),
        P("tp", ("dp", "kv")),
        P("dp"),
        P(("dp", "kv"), None, "tp"),
        P(("dp", "kv"), None, "tp"),
        P(("dp", "kv"), "tp", None),
        P(("dp", "kv")),
    )
    out_specs = (P(("dp", "kv"), "tp"), P(("dp", "kv"), "tp"))
    return jax.shard_map(
        per_device, mesh=mesh, in_specs=in_specs, out_specs=out_specs, check_vma=False
    )
```

profile of v0, /device:TPU:0, one launch (start us, length us, event | category | flops | bytes accessed | tf_op | source)
XLA Modules:
  0.0 125.6 jit_solution(8513010429715983522)
XLA Ops:
  0.7 1.4 %fusion.9 = f32[129]{0:T(256)S(1)} fusion(bf16[1,2048]{1,0:T(2,128)(2,1)} %param.20, bf16[128,2048]{1,0:T(8,128)(2,1)} %param.19), kind=kLoop, calls=%fused_computation.16 | loop fusion | flops 1585023 | bytes 528900 | tf_op jit(solution)/shard_map/reduce_sum | solution.py:24
  2.2 0.7 dynamic_slice.18
  2.9 1.5 %fusion.25 = f32[129,8]{0,1:T(8,128)S(1)} fusion(bf16[2048,16]{0,1:T(8,128)(2,1)} %param.25, s32[]{:T(128)S(6)} %select_n.43, f32[8]{0:T(128)S(1)} %dynamic_slice.18, f32[2048]{0:T(1024)} %param.21, f32[129]{0:T(256)S(1)} %add_rsqrt_fusion, bf16[1,2048]{1,0:T(2,128)(2,1)} %param.20, bf16[128,2048]{1,0:T(8,128)(2,1)} %param.19), kind=kOutput, calls=%fused_computation.49 | convolution fusion | flops 6085704 | bytes 578120 | tf_op jit(solution)/shard_map/dot_general | solution.py:128
  4.5 0.7 dynamic-slice
  5.8 0.2 dynamic-update-slice
  6.1 13.5 %all-reduce.1 = f32[32]{0:T(128)S(1)} all-reduce(f32[32]{0:T(128)S(1)} %dynamic-update-slice), channel_id=2, replica_groups=mesh['dp'=4,'kv'=4,'tp'=2] {'kv'}, use_global_device_ids=true, to_apply=%add.1 | all-reduce | flops 32 | bytes 256
  19.8 0.2 reduce_window_sum.34
  20.3 2.1 %convolution_convert_fusion.2 = bf16[129,512]{1,0:T(8,128)(2,1)S(1)} fusion(bf16[2048,512]{1,0:T(8,128)(2,1)} %param.23, f32[2048]{0:T(1024)S(1)} %copy-done.20, f32[129]{0:T(256)S(1)} %add_rsqrt_fusion, bf16[1,2048]{1,0:T(2,128)(2,1)S(1)} %copy-done.13, bf16[128,2048]{1,0:T(8,128)(2,1)S(1)} %copy-done.3), kind=kOutput, calls=%fused_computation.14 | convolution fusion | flops 272448000 | bytes 2766340 | tf_op jit(solution)/shard_map/dot_general | solution.py:120
  22.4 1.1 copy.123
  23.5 2.3 %convolution_convert_fusion.3 = bf16[129,512]{1,0:T(8,128)(2,1)S(1)} fusion(bf16[2048,512]{1,0:T(8,128)(2,1)} %param.22, f32[2048]{0:T(1024)S(1)} %copy-done.20, f32[129]{0:T(256)S(1)} %add_rsqrt_fusion, bf16[1,2048]{1,0:T(2,128)(2,1)S(1)} %copy-done.13, bf16[128,2048]{1,0:T(8,128)(2,1)} %param.19), kind=kOutput, calls=%fused_computation.15 | convolution fusion | flops 272448000 | bytes 2766340 | tf_op jit(solution)/shard_map/dot_general | solution.py:119
  25.8 0.6 copy-done.7
  26.5 14.8 %all_gather.12 = bf16[512,512]{1,0:T(8,128)(2,1)S(1)} all-gather(bf16[128,512]{1,0:T(8,128)(2,1)S(1)} %slice.52), channel_id=1, replica_groups=mesh['dp'=4,'kv'=4,'tp'=2] {'kv'}, dimensions={0}, use_global_device_ids=true | all-gather | bytes 655360 | tf_op jit(solution)/shard_map/all_gather | solution.py:142
  41.2 0.2 copy.122
  41.6 3.8 %fusion.2 = (f32[8,512]{1,0:T(8,128)S(1)}, f32[8,512,640]{2,1,0:T(8,128)S(1)}) fusion(f32[8,640]{1,0:T(8,128)S(1)} %maximum_negate_fusion, pred[512,640]{1,0:T(8,128)(4,1)S(1)} %concatenate.22, bf16[512,8,64]{0,2,1:T(8,128)(2,1)S(1)} %bitcast.94, bf16[640,8,64]{0,2,1:T(8,128)(2,1)} %bitcast.91), kind=kOutput, calls=%fused_computation.6 | convolution fusion | flops 346025984 | bytes 12029952 | tf_op jit(solution)/shard_map/qhd,khd->hqk/dot_general | solution.py:40
  45.4 2.9 %fusion.1 = f32[8,512]{1,0:T(8,128)S(1)} fusion(f32[8,512,640]{2,1,0:T(8,128)S(1)} %get-tuple-element.116, f32[8,512]{1,0:T(8,128)S(1)} %get-tuple-element.115, f32[8,640]{1,0:T(8,128)S(1)} %maximum_negate_fusion, pred[512,640]{1,0:T(8,128)(4,1)S(1)} %concatenate.22), kind=kLoop, calls=%fused_computation.5 | loop fusion | flops 13103104 | bytes 10866688 | tf_op jit(solution)/shard_map/reduce_sum | solution.py:56
  48.3 1.1 copy-done.1
  49.5 0.6 broadcast.115
  50.0 1.3 %reduce.22 = f32[512,8]{1,0:T(8,128)S(1)} reduce(f32[512,1,8]{2,1,0:T(1,128)S(1)} %bitcast.87, f32[]{:T(128)} %broadcast.115), dimensions={1}, to_apply=%bitcast.60.reduce_sub_computation | reduce | bytes 32772
  51.4 0.8 reshape.272
  52.1 4.0 %all-to-all-start = ((f32[4,1,1024]{2,1,0:T(1,128)}), f32[4,1,1024]{2,1,0:T(1,128)}, u32[]{:S(2)}, u32[]{:S(2)}) async-start(f32[4,1,1024]{2,1,0:T(1,128)} %reshape.272), calls=%async_computation | async-start | bytes 32768 | tf_op jit(solution)/shard_map/all_to_all | solution.py:150
  56.2 0.7 slice_reduce_fusion.1
  57.6 2.3 %reduce-window.6 = f32[1,8,8,128]{3,2,1,0:T(8,128)S(1)} reduce-window(f32[1,8,8,128]{3,2,1,0:T(8,128)S(1)} %copy.135, f32[]{:T(128)} %constant.56.clone.1), window={size=1x1x1x128 pad=0_0x0_0x0_0x127_0}, to_apply=%region_10.11 | reduce-window | flops 1040384 | bytes 65540 | tf_op jit(solution)/shard_map/reduce-window
  59.9 0.2 slice_reduce_fusion
  60.0 1.0 copy.148
  61.0 0.7 slice_reduce_fusion.3
  61.9 1.3 %slice_reduce_fusion.2 = bf16[512]{0:T(512)(128)(2,1)} fusion(bf16[129,512]{1,0:T(8,128)(2,1)} %copy-done.6), kind=kLoop, calls=%fused_computation.58 | loop fusion | bytes 2048 | tf_op jit(solution)/shard_map/slice | solution.py:155
  63.2 2.1 %convolution_convert_fusion.1 = bf16[129,512]{1,0:T(8,128)(2,1)S(1)} fusion(bf16[2048,512]{1,0:T(8,128)(2,1)} %param.24, f32[2048]{0:T(1024)} %param.21, f32[129]{0:T(256)} %copy-done.18, bf16[1,2048]{1,0:T(2,128)(2,1)} %param.20, bf16[128,2048]{1,0:T(8,128)(2,1)S(1)} %copy-done.4), kind=kOutput, calls=%fused_computation.13 | convolution fusion | flops 272448000 | bytes 2766340 | tf_op jit(solution)/shard_map/dot_general | solution.py:121
  65.3 0.6 copy-done.5
  66.0 1.1 pad_maximum_fusion.1
  67.1 1.1 copy.129
  68.2 0.2 reduce-window.9
  68.5 1.5 %copy.134 = bf16[1,1024,512]{1,2,0:T(8,128)(2,1)S(1)} copy(bf16[1,1024,512]{2,1,0:T(8,128)(2,1)} %param.32) | data formatting | bytes 2097152 | tf_op args[13]
  69.9 1.3 %reshape.238 = bf16[8,64]{1,0:T(8,128)(2,1)} reshape(bf16[512]{0:T(512)(128)(2,1)} %slice_reduce_fusion.2) | data formatting | bytes 2048 | tf_op jit(solution)/shard_map/reshape.34
  71.3 6.7 %divide_convert_fusion = bf16[512,8,64]{0,2,1:T(8,128)(2,1)} fusion(bf16[640,8,64]{0,2,1:T(8,128)(2,1)} %bitcast.90, f32[8,512,640]{2,1,0:T(8,128)} %copy-done.1, f32[8,512]{1,0:T(8,128)S(1)} %get-tuple-element.115, f32[8,640]{1,0:T(8,128)S(1)} %copy-done.9, pred[512,640]{1,0:T(8,128)(4,1)S(1)} %concatenate.22, f32[512,8]{0,1:T(8,128)} %bitcast.99), kind=kOutput, calls=%fused_computation.22 | convolution fusion | flops 349175808 | bytes 12046336 | tf_op jit(solution)/shard_map/hqk,khd->qhd/dot_general | solution.py:57
  78.0 0.7 fusion.30
  78.6 0.2 fusion.42
  79.0 0.2 fusion.40
  79.2 0.2 fusion.22
  79.6 1.3 %reduce.24 = f32[512,8]{1,0:T(8,128)S(1)} reduce(f32[512,1,8]{2,1,0:T(1,128)S(1)} %bitcast.88, f32[]{:T(128)} %broadcast.115), dimensions={1}, to_apply=%bitcast.62.reduce_sub_computation | reduce | bytes 32772
  80.9 0.8 reshape.274
  81.7 4.9 %all-to-all-start.1 = ((f32[4,1,1024]{2,1,0:T(1,128)}), f32[4,1,1024]{2,1,0:T(1,128)S(1)}, u32[]{:S(2)}, u32[]{:S(2)}) async-start(f32[4,1,1024]{2,1,0:T(1,128)} %reshape.274), calls=%async_computation.1 | async-start | bytes 32768 | tf_op jit(solution)/shard_map/all_to_all | solution.py:149
  86.5 2.4 %copy.130 = bf16[1,512,512]{2,0,1:T(2,128)(2,1)S(1)} copy(bf16[1,512,512]{1,2,0:T(8,128)(2,1)} %bitcast.92) | data formatting | bytes 1048576 | tf_op jit(solution)/shard_map/broadcast_in_dim;reshape | solution.py:147
  89.0 0.5 broadcast.114
  89.5 4.6 %reduce.21 = bf16[512,512]{1,0:T(8,128)(2,1)} reduce(bf16[512,1,512]{2,1,0:T(2,128)(2,1)S(1)} %bitcast.82, bf16[]{:T(256)} %broadcast.114), dimensions={1}, to_apply=%bitcast.58.reduce_sub_computation | reduce | bytes 1048578
  94.1 2.2 %reshape.270 = bf16[4,2,32768]{2,1,0:T(2,128)(2,1)} reshape(bf16[512,512]{1,0:T(8,128)(2,1)} %reduce.21) | data formatting | bytes 1048576
  96.3 1.5 %copy.139 = bf16[1,1024,512]{1,2,0:T(8,128)(2,1)S(1)} copy(bf16[1,1024,512]{2,1,0:T(8,128)(2,1)} %param.33) | data formatting | bytes 2097152 | tf_op args[14]
  97.8 5.1 %all-to-all-start.2 = ((bf16[4,2,32768]{2,1,0:T(2,128)(2,1)}), bf16[4,2,32768]{2,1,0:T(2,128)(2,1)}, u32[]{:S(2)}, u32[]{:S(2)}) async-start(bf16[4,2,32768]{2,1,0:T(2,128)(2,1)} %reshape.270), calls=%async_computation.2 | async-start | bytes 1048576 | tf_op jit(solution)/shard_map/all_to_all | solution.py:147
  102.9 0.7 fusion.29
  103.7 0.4 fusion.19
  104.2 0.3 reshape.257
  104.5 1.4 %reduce.23 = f32[4,1024]{1,0:T(4,128)S(1)} reduce(f32[4,1,1024]{2,1,0:T(1,128)} %all-to-all-done, f32[]{:T(128)} %broadcast.115), dimensions={1}, to_apply=%all_to_all.10.reduce_sub_computation | reduce | bytes 32772 | tf_op jit(solution)/shard_map/all_to_all | solution.py:150
  105.9 0.4 reshape.273
  106.3 0.7 reduce.25
  107.1 0.4 reshape.275
  107.8 5.5 %all-to-all-done.2 = bf16[4,2,32768]{2,1,0:T(2,128)(2,1)} async-done(((bf16[4,2,32768]{2,1,0:T(2,128)(2,1)}), bf16[4,2,32768]{2,1,0:T(2,128)(2,1)}, u32[]{:S(2)}, u32[]{:S(2)}) %all-to-all-start.2) | async-done | bytes 524320 | tf_op jit(solution)/shard_map/all_to_all | solution.py:147
  113.3 2.2 %reshape.271 = bf16[512,1,512]{2,1,0:T(2,128)(2,1)S(1)} reshape(bf16[4,2,32768]{2,1,0:T(2,128)(2,1)} %all-to-all-done.2) | data formatting | bytes 1048576
  115.5 1.1 copy_convert_fusion
  116.6 2.6 %copy.132 = f32[1,512,512]{1,2,0:T(8,128)} copy(f32[1,512,512]{2,1,0:T(8,128)} %copy_convert_fusion) | data formatting | bytes 2097152 | tf_op jit(solution)/shard_map/convert_element_type | solution.py:87
  119.2 1.6 %reshape.241 = f32[4,128,8,64]{1,0,3,2:T(4,128)S(1)} reshape(f32[1,512,512]{1,2,0:T(8,128)} %copy.132) | data formatting | bytes 2097152 | tf_op jit(solution)/shard_map/convert_element_type | solution.py:87
  120.8 0.7 multiply_reduce_fusion
  121.6 2.2 %all_gather.15 = bf16[129,1024]{0,1:T(8,128)(2,1)S(1)} all-gather(bf16[129,512]{0,1:T(8,128)(2,1)S(1)} %pad_maximum_fusion.3), channel_id=1, replica_groups=mesh['dp'=4,'kv'=4,'tp'=2] {'tp'}, dimensions={1}, use_global_device_ids=true | all-gather | bytes 396288 | tf_op jit(solution)/shard_map/all_gather | solution.py:196
  123.8 0.5 convolution_convert_fusion
  124.3 0.7 slice.63
  125.0 0.6 slice.64
  (85 shorter events, 2.1 us)
Async XLA Ops:
  0.6 123.1 %copy-start = (bf16[1024,1024]{1,0:T(8,128)(2,1)S(1)}, bf16[1024,1024]{1,0:T(8,128)(2,1)}, u32[]{:S(2)}) copy-start(bf16[1024,1024]{1,0:T(8,128)(2,1)} %param.27) | copy-start | bytes 6291460
  0.6 3.8 %copy-start.21 = (u32[32]{0:T(128)S(1)}, u32[32]{0:T(128)}, u32[]{:S(2)}) copy-start(u32[32]{0:T(128)} %constant.74) | copy-start | bytes 388
  0.7 19.6 %copy-start.3 = (bf16[128,2048]{1,0:T(8,128)(2,1)S(1)}, bf16[128,2048]{1,0:T(8,128)(2,1)}, u32[]{:S(2)}) copy-start(bf16[128,2048]{1,0:T(8,128)(2,1)} %param.19) | copy-start | bytes 1572868
  0.7 19.6 %copy-start.13 = (bf16[1,2048]{1,0:T(2,128)(2,1)S(1)}, bf16[1,2048]{1,0:T(2,128)(2,1)}, u32[]{:S(2)}) copy-start(bf16[1,2048]{1,0:T(2,128)(2,1)} %param.20) | copy-start | bytes 12292
  0.7 19.6 %copy-start.20 = (f32[2048]{0:T(1024)S(1)}, f32[2048]{0:T(1024)}, u32[]{:S(2)}) copy-start(f32[2048]{0:T(1024)} %param.21) | copy-start | bytes 24580
  0.7 19.3 %copy-start.19 = (f32[16]{0:T(128)S(1)}, f32[16]{0:T(128)}, u32[]{:S(2)}) copy-start(f32[16]{0:T(128)} %param.31) | copy-start | bytes 196
  2.1 21.4 %copy-start.18 = (f32[129]{0:T(256)}, f32[129]{0:T(256)S(1)}, u32[]{:S(2)}) copy-start(f32[129]{0:T(256)S(1)} %add_rsqrt_fusion) | copy-start | bytes 1552
  19.7 2.7 %copy-start.2 = (bf16[512,512]{1,0:T(8,128)(2,1)S(1)}, bf16[512,512]{1,0:T(8,128)(2,1)}, u32[]{:S(2)}) copy-start(bf16[512,512]{1,0:T(8,128)(2,1)} %param.28) | copy-start | bytes 1572868
  22.3 3.5 %copy-start.6 = (bf16[129,512]{1,0:T(8,128)(2,1)}, bf16[129,512]{1,0:T(8,128)(2,1)S(1)}, u32[]{:S(2)}) copy-start(bf16[129,512]{1,0:T(8,128)(2,1)S(1)} %convolution_convert_fusion.2) | copy-start | bytes 396292
  23.5 17.9 %copy-start.12 = (f32[8,512]{1,0:T(8,128)S(1)}, f32[8,512]{1,0:T(8,128)}, u32[]{:S(2)}) copy-start(f32[8,512]{1,0:T(8,128)} %param.30) | copy-start | bytes 49156
  25.8 0.7 copy-start.7
  41.5 3.9 %copy-start.8 = (f32[8,640]{1,0:T(8,128)}, f32[8,640]{1,0:T(8,128)S(1)}, u32[]{:S(2)}) copy-start(f32[8,640]{1,0:T(8,128)S(1)} %maximum_negate_fusion) | copy-start | bytes 61444
  45.3 4.0 %copy-start.1 = (f32[8,512,640]{2,1,0:T(8,128)}, f32[8,512,640]{2,1,0:T(8,128)S(1)}, u32[]{:S(2)}) copy-start(f32[8,512,640]{2,1,0:T(8,128)S(1)} %get-tuple-element.116) | copy-start | bytes 31457284
  45.4 12.2 %copy-start.11 = (f32[1,8,1024]{2,1,0:T(8,128)S(1)}, f32[1,8,1024]{2,1,0:T(8,128)}, u32[]{:S(2)}) copy-start(f32[1,8,1024]{2,1,0:T(8,128)} %param.34) | copy-start | bytes 98308
  45.4 17.8 %copy-start.4 = (bf16[128,2048]{1,0:T(8,128)(2,1)S(1)}, bf16[128,2048]{1,0:T(8,128)(2,1)}, u32[]{:S(2)}) copy-start(bf16[128,2048]{1,0:T(8,128)(2,1)} %param.19) | copy-start | bytes 1572868
  49.3 8.2 %copy-start.10 = (f32[8,512]{1,0:T(8,128)}, f32[8,512]{1,0:T(8,128)S(1)}, u32[]{:S(2)}) copy-start(f32[8,512]{1,0:T(8,128)S(1)} %fusion.1) | copy-start | bytes 49156
  52.1 29.5 %all-to-all-start = ((f32[4,1,1024]{2,1,0:T(1,128)}), f32[4,1,1024]{2,1,0:T(1,128)}, u32[]{:S(2)}, u32[]{:S(2)}) async-start(f32[4,1,1024]{2,1,0:T(1,128)} %reshape.272), calls=%async_computation | async-start | bytes 32768 | tf_op jit(solution)/shard_map/all_to_all | solution.py:150
  57.5 7.8 %copy-start.15 = (pred[1024]{0:T(1024)(128)(4,1)}, pred[1024]{0:T(1024)(128)(4,1)S(1)}, u32[]{:S(2)}) copy-start(pred[1024]{0:T(1024)(128)(4,1)S(1)} %iota_compare_fusion.1) | copy-start | bytes 3076
  65.3 0.7 copy-start.5
  66.0 5.2 %copy-start.9 = (f32[8,640]{1,0:T(8,128)S(1)}, f32[8,640]{1,0:T(8,128)}, u32[]{:S(2)}) copy-start(f32[8,640]{1,0:T(8,128)} %copy-done.8) | copy-start | bytes 61444
  71.2 7.6 %copy-start.14 = (bf16[8,64]{1,0:T(8,128)(2,1)S(1)}, bf16[8,64]{1,0:T(8,128)(2,1)}, u32[]{:S(2)}) copy-start(bf16[8,64]{1,0:T(8,128)(2,1)} %reshape.238) | copy-start | bytes 3076
  71.2 7.8 %copy-start.16 = (pred[1024]{0:T(1024)(128)(4,1)S(1)}, pred[1024]{0:T(1024)(128)(4,1)}, u32[]{:S(2)}) copy-start(pred[1024]{0:T(1024)(128)(4,1)} %copy-done.15) | copy-start | bytes 3076
  71.2 7.8 %copy-start.17 = (f32[8]{0:T(128)S(1)}, f32[8]{0:T(128)}, u32[]{:S(2)}) copy-start(f32[8]{0:T(128)} %slice_reduce_fusion.1) | copy-start | bytes 100
  81.7 16.1 %all-to-all-start.1 = ((f32[4,1,1024]{2,1,0:T(1,128)}), f32[4,1,1024]{2,1,0:T(1,128)S(1)}, u32[]{:S(2)}, u32[]{:S(2)}) async-start(f32[4,1,1024]{2,1,0:T(1,128)} %reshape.274), calls=%async_computation.1 | async-start | bytes 32768 | tf_op jit(solution)/shard_map/all_to_all | solution.py:149
  97.8 15.5 %all-to-all-start.2 = ((bf16[4,2,32768]{2,1,0:T(2,128)(2,1)}), bf16[4,2,32768]{2,1,0:T(2,128)(2,1)}, u32[]{:S(2)}, u32[]{:S(2)}) async-start(bf16[4,2,32768]{2,1,0:T(2,128)(2,1)} %reshape.270), calls=%async_computation.2 | async-start | bytes 1048576 | tf_op jit(solution)/shard_map/all_to_all | solution.py:147
where the time goes:
time: 127 us; the launch traced here: 126 us
  local copies, waits for them, and re-layouts  31.8 us (25%)
  blocking collectives  30.4 us (24%)
  other arithmetic  21.8 us (17%)
  matrix products  19.5 us (15%)
  starting transfers between devices  14 us (11%)
  waiting for transfers between devices  5.55 us (4%)
  between operations  2.56 us (2%)
    all_gather x1, blocking collectives, per_device(): gathered = lax.all_gather(own_queries, 'kv', axis=0, tiled=True)  14.8 us
    unnamed x57, local copies, waits for them, and re-layouts  14.3 us
    unnamed x1, blocking collectives  13.5 us
    unnamed x4, other arithmetic  7.29 us
    dot_general x1, matrix products, one_block(): jnp.einsum('hqk,khd->qhd', exp_scores.astype(jnp.bfloat16), value_heads,...  6.67 us
    all_to_all x1, waiting for transfers between devices, per_device(): lax.all_to_all(part_means[None], 'kv', split_axis=1, concat_axis=0, tiled...  5.54 us
    all_to_all x1, starting transfers between devices, per_device(): lax.all_to_all(part_means[None], 'kv', split_axis=1, concat_axis=0, tiled...  5.1 us
    all_to_all x1, starting transfers between devices, per_device(): lax.all_to_all(part_high[None], 'kv', split_axis=1, concat_axis=0, tiled=...  4.87 us
  transfers between devices with their start and end apart: 3, of which 1 were waited for; matrix products, arithmetic and copies ran while one was open for 32% of the time, Pallas kernels for 0%

commit v1 on v0

--- a/solution.py
+++ b/solution.py
@@ -144,7 +144,10 @@
     part_means, part_high, part_mass = attend_piece(
         gathered, positions, all_keys, all_values, key_bias, key_slots, cache_len
     )
-    part_means = lax.all_to_all(part_means[None], "kv", split_axis=1, concat_axis=0, tiled=True)
+    own = part_means[None]
+    parts = jnp.split(own, lax.axis_size("kv"), axis=1)
+    received = lax.all_to_all(jnp.stack(parts), "kv", 0, 0)
+    part_means = jnp.concatenate(received, axis=0)
     part_high, part_mass = (
         lax.all_to_all(part_high[None], "kv", split_axis=1, concat_axis=0, tiled=True),
         lax.all_to_all(part_mass[None], "kv", split_axis=1, concat_axis=0, tiled=True),

time: 127 us -> 109 us (0.86)
  local copies, waits for them, and re-layouts: 31.8 us -> 20.5 us
  other arithmetic: 21.8 us -> 18.7 us
  starting transfers between devices: 14 us -> 11.9 us
  waiting for transfers between devices: 5.55 us -> 3.49 us
    unnamed x4 -> x3, other arithmetic: 7.29 us -> 2.68 us
    unnamed x57 -> x34, local copies, waits for them, and re-layouts: 14.3 us -> 10.1 us
    convert_element_type x2 -> x0, local copies, waits for them, and re-layouts: 4.16 us -> none  [combine(): part_means.reshape(peer_count, row_count, head_count, -1)]
    all_to_all x1, waiting for transfers between devices: 5.54 us -> 2 us  [per_device(): received = lax.all_to_all(jnp.stack(parts), 'kv', 0, 0)]
    another operation x8, local copies, waits for them, and re-layouts: 5.01 us -> 2.17 us
    another operation x2 -> x3, other arithmetic: 2.43 us -> 4.28 us
    all_to_all x1, starting transfers between devices: 5.1 us -> 3.61 us  [per_device(): received = lax.all_to_all(jnp.stack(parts), 'kv', 0, 0)]
    all_to_all x1, waiting for transfers between devices: 0.01 us -> 1.48 us  [per_device(): lax.all_to_all(part_high[None], 'kv', split_axis=1, concat_axis=0, tiled=...]
  transfers between devices with their start and end apart: 3 -> 3, of which waited for: 1 -> 2; matrix products, arithmetic and copies ran while one was open for 32% -> 31% of each run, Pallas kernels for 0% -> 0%
where the time goes in v1:
time: 109 us; the launch traced here: 108 us
  blocking collectives  30.4 us (28%)
  local copies, waits for them, and re-layouts  20.5 us (19%)
  matrix products  20.3 us (19%)
  other arithmetic  18.7 us (17%)
  starting transfers between devices  11.9 us (11%)
  waiting for transfers between devices  3.49 us (3%)
  between operations  2.36 us (2%)
    all_gather x1, blocking collectives, per_device(): gathered = lax.all_gather(own_queries, 'kv', axis=0, tiled=True)  14.8 us
    unnamed x1, blocking collectives  13.5 us
    unnamed x34, local copies, waits for them, and re-layouts  10.1 us
    dot_general x1, matrix products, one_block(): jnp.einsum('hqk,khd->qhd', exp_scores.astype(jnp.bfloat16), value_heads,...  5.96 us
    all_to_all x1, starting transfers between devices, per_device(): lax.all_to_all(part_high[None], 'kv', split_axis=1, concat_axis=0, tiled=...  4.87 us
    dot_general x1, matrix products, one_block(): jnp.einsum('qhd,khd->hqk', block_q.reshape(row_count, head_count, head_wi...  3.9 us
    all_to_all x1, starting transfers between devices, per_device(): received = lax.all_to_all(jnp.stack(parts), 'kv', 0, 0)  3.61 us
    all_to_all x1, starting transfers between devices, per_device(): lax.all_to_all(part_mass[None], 'kv', split_axis=1, concat_axis=0, tiled=...  3.43 us
  transfers between devices with their start and end apart: 3, of which 2 were waited for; matrix products, arithmetic and copies ran while one was open for 31% of the time, Pallas kernels for 0%

profile of v1, /device:TPU:0, one launch (start us, length us, event | category | flops | bytes accessed | tf_op | source)
XLA Modules:
  0.0 107.7 jit_solution(11430982527838824378)
XLA Ops:
  0.7 1.4 %fusion.9 = f32[129]{0:T(256)S(1)} fusion(bf16[1,2048]{1,0:T(2,128)(2,1)} %param.20, bf16[128,2048]{1,0:T(8,128)(2,1)} %param.19), kind=kLoop, calls=%fused_computation.16 | loop fusion | flops 1585023 | bytes 528900 | tf_op jit(solution)/shard_map/reduce_sum | solution.py:24
  2.1 0.7 dynamic_slice.18
  2.9 1.5 %fusion.26 = f32[129,8]{0,1:T(8,128)S(1)} fusion(bf16[2048,16]{0,1:T(8,128)(2,1)} %param.25, s32[]{:T(128)S(6)} %select_n.43, f32[8]{0:T(128)S(1)} %dynamic_slice.18, f32[2048]{0:T(1024)} %param.21, f32[129]{0:T(256)S(1)} %add_rsqrt_fusion, bf16[1,2048]{1,0:T(2,128)(2,1)} %param.20, bf16[128,2048]{1,0:T(8,128)(2,1)} %param.19), kind=kOutput, calls=%fused_computation.54 | convolution fusion | flops 6085704 | bytes 578120 | tf_op jit(solution)/shard_map/dot_general | solution.py:128
  4.3 0.1 slice_reduce_fusion.4
  4.5 0.6 dynamic-slice
  5.7 0.2 dynamic-update-slice
  5.9 13.5 %all-reduce.1 = f32[32]{0:T(128)S(1)} all-reduce(f32[32]{0:T(128)S(1)} %dynamic-update-slice), channel_id=2, replica_groups=mesh['dp'=4,'kv'=4,'tp'=2] {'kv'}, use_global_device_ids=true, to_apply=%add.1 | all-reduce | flops 32 | bytes 256
  19.7 0.2 reduce_window_sum.34
  20.1 2.1 %convolution_convert_fusion.2 = bf16[129,512]{1,0:T(8,128)(2,1)S(1)} fusion(bf16[2048,512]{1,0:T(8,128)(2,1)} %param.23, f32[2048]{0:T(1024)S(1)} %copy-done.10, f32[129]{0:T(256)S(1)} %add_rsqrt_fusion, bf16[1,2048]{1,0:T(2,128)(2,1)S(1)} %copy-done.8, bf16[128,2048]{1,0:T(8,128)(2,1)S(1)} %copy-done.3), kind=kOutput, calls=%fused_computation.14 | convolution fusion | flops 272448000 | bytes 2766340 | tf_op jit(solution)/shard_map/dot_general | solution.py:120
  22.3 1.1 copy.67
  23.4 2.3 %convolution_convert_fusion.3 = bf16[129,512]{1,0:T(8,128)(2,1)S(1)} fusion(bf16[2048,512]{1,0:T(8,128)(2,1)} %param.22, f32[2048]{0:T(1024)S(1)} %copy-done.10, f32[129]{0:T(256)S(1)} %add_rsqrt_fusion, bf16[1,2048]{1,0:T(2,128)(2,1)S(1)} %copy-done.8, bf16[128,2048]{1,0:T(8,128)(2,1)} %param.19), kind=kOutput, calls=%fused_computation.15 | convolution fusion | flops 272448000 | bytes 2766340 | tf_op jit(solution)/shard_map/dot_general | solution.py:119
  25.7 0.6 copy-done.5
  26.3 14.8 %all_gather.12 = bf16[512,512]{1,0:T(8,128)(2,1)S(1)} all-gather(bf16[128,512]{1,0:T(8,128)(2,1)S(1)} %slice.52), channel_id=1, replica_groups=mesh['dp'=4,'kv'=4,'tp'=2] {'kv'}, dimensions={0}, use_global_device_ids=true | all-gather | bytes 655360 | tf_op jit(solution)/shard_map/all_gather | solution.py:142
  41.1 1.0 copy.66
  42.2 3.9 %fusion.2 = (f32[8,512]{1,0:T(8,128)S(1)}, f32[8,512,640]{2,1,0:T(8,128)S(1)}) fusion(f32[8,640]{1,0:T(8,128)S(1)} %maximum_negate_fusion, pred[512,640]{1,0:T(8,128)(4,1)S(1)} %concatenate.22, bf16[512,8,64]{0,2,1:T(8,128)(2,1)} %bitcast.100, bf16[640,8,64]{0,2,1:T(8,128)(2,1)} %bitcast.97), kind=kOutput, calls=%fused_computation.6 | convolution fusion | flops 346025984 | bytes 12029952 | tf_op jit(solution)/shard_map/qhd,khd->hqk/dot_general | solution.py:40
  46.1 2.9 %fusion.1 = f32[8,512]{1,0:T(8,128)S(1)} fusion(f32[8,512,640]{2,1,0:T(8,128)S(1)} %get-tuple-element.120, f32[8,512]{1,0:T(8,128)S(1)} %get-tuple-element.119, f32[8,640]{1,0:T(8,128)S(1)} %maximum_negate_fusion, pred[512,640]{1,0:T(8,128)(4,1)S(1)} %concatenate.22), kind=kLoop, calls=%fused_computation.5 | loop fusion | flops 13103104 | bytes 10866688 | tf_op jit(solution)/shard_map/reduce_sum | solution.py:56
  49.0 1.1 %copy-done.1 = f32[8,512,640]{2,1,0:T(8,128)} copy-done((f32[8,512,640]{2,1,0:T(8,128)}, f32[8,512,640]{2,1,0:T(8,128)S(1)}, u32[]{:S(2)}) %copy-start.1) | copy-done | bytes 10485784
  50.1 0.1 copy.70
  50.2 0.6 broadcast.110
  50.8 1.3 %reduce.20 = f32[512,8]{1,0:T(8,128)S(1)} reduce(f32[512,1,8]{2,1,0:T(1,128)S(1)} %bitcast.94, f32[]{:T(128)} %broadcast.110), dimensions={1}, to_apply=%bitcast.68.reduce_sub_computation | reduce | bytes 32772
  52.2 0.8 reshape.251
  52.9 3.4 %all-to-all-start = ((f32[4,1,1024]{2,1,0:T(1,128)}), f32[4,1,1024]{2,1,0:T(1,128)S(1)}, u32[]{:S(2)}, u32[]{:S(2)}) async-start(f32[4,1,1024]{2,1,0:T(1,128)} %reshape.251), calls=%async_computation | async-start | bytes 32768 | tf_op jit(solution)/shard_map/all_to_all | solution.py:153
  56.4 0.1 slice_reduce_fusion.1
  57.2 2.3 %reduce-window.6 = f32[1,8,8,128]{3,2,1,0:T(8,128)S(1)} reduce-window(f32[1,8,8,128]{3,2,1,0:T(8,128)S(1)} %copy.76, f32[]{:T(128)} %constant.56.clone.1), window={size=1x1x1x128 pad=0_0x0_0x0_0x127_0}, to_apply=%region_10.11 | reduce-window | flops 1040384 | bytes 65540 | tf_op jit(solution)/shard_map/reduce-window
  59.5 0.2 slice_reduce_fusion
  59.6 1.0 copy.89
  60.6 0.7 slice_reduce_fusion.3
  61.6 2.3 %convolution_convert_fusion.1 = bf16[129,512]{1,0:T(8,128)(2,1)S(1)} fusion(bf16[2048,512]{1,0:T(8,128)(2,1)} %param.24, f32[2048]{0:T(1024)S(1)} %copy-done.10, f32[129]{0:T(256)S(1)} %add_rsqrt_fusion, bf16[1,2048]{1,0:T(2,128)(2,1)S(1)} %copy-done.8, bf16[128,2048]{1,0:T(8,128)(2,1)} %param.19), kind=kOutput, calls=%fused_computation.13 | convolution fusion | flops 272448000 | bytes 2766340 | tf_op jit(solution)/shard_map/dot_general | solution.py:121
  63.8 0.6 copy-done.4
  64.5 1.1 %pad_maximum_fusion.1 = bf16[640,512]{1,0:T(8,128)(2,1)S(1)} fusion(bf16[128,512]{1,0:T(8,128)(2,1)S(1)} %slice.55, bf16[512,512]{1,0:T(8,128)(2,1)} %param.29), kind=kLoop, calls=%fused_computation.24 | loop fusion | flops 1310720 | bytes 1310720 | tf_op jit(solution)/shard_map/concatenate | solution.py:137
  65.6 1.1 %copy.73 = bf16[640,512]{0,1:T(8,128)(2,1)} copy(bf16[640,512]{1,0:T(8,128)(2,1)S(1)} %pad_maximum_fusion.1) | data formatting | bytes 1310720 | tf_op jit(solution)/shard_map/concatenate | solution.py:137
  66.7 6.0 %divide_convert_fusion = bf16[512,8,64]{0,2,1:T(8,128)(2,1)S(1)} fusion(bf16[640,8,64]{0,2,1:T(8,128)(2,1)} %bitcast.98, f32[8,512,640]{2,1,0:T(8,128)} %copy-done.1, f32[8,512]{1,0:T(8,128)S(1)} %get-tuple-element.119, f32[8,640]{1,0:T(8,128)S(1)} %maximum_negate_fusion, pred[512,640]{1,0:T(8,128)(4,1)S(1)} %concatenate.22, f32[512,8]{0,1:T(8,128)S(1)} %bitcast.105), kind=kOutput, calls=%fused_computation.22 | convolution fusion | flops 349175808 | bytes 12046336 | tf_op jit(solution)/shard_map/hqk,khd->qhd/dot_general | solution.py:57
  72.7 0.8 slice_bitcast_fusion.3
  73.4 0.2 reduce-window.9
  73.7 1.5 %copy.75 = bf16[1,1024,512]{1,2,0:T(8,128)(2,1)S(1)} copy(bf16[1,1024,512]{2,1,0:T(8,128)(2,1)} %param.32) | data formatting | bytes 2097152 | tf_op args[13]
  75.3 0.7 fusion.31
  76.0 0.2 fusion.43
  76.2 0.1 fusion.29
  76.3 0.2 fusion.41
  76.5 0.2 fusion.23
  76.8 0.1 copy.71
  76.9 1.3 %reduce.22 = f32[512,8]{1,0:T(8,128)S(1)} reduce(f32[512,1,8]{2,1,0:T(1,128)S(1)} %bitcast.95, f32[]{:T(128)} %broadcast.110), dimensions={1}, to_apply=%bitcast.70.reduce_sub_computation | reduce | bytes 32772
  78.2 0.8 reshape.253
  79.0 4.9 %all-to-all-start.1 = ((f32[4,1,1024]{2,1,0:T(1,128)}), f32[4,1,1024]{2,1,0:T(1,128)S(1)}, u32[]{:S(2)}, u32[]{:S(2)}) async-start(f32[4,1,1024]{2,1,0:T(1,128)} %reshape.253), calls=%async_computation.1 | async-start | bytes 32768 | tf_op jit(solution)/shard_map/all_to_all | solution.py:152
  83.9 1.9 %pad_maximum_fusion.3 = bf16[4,1,128,512]{2,3,1,0:T(8,128)(2,1)} fusion(bf16[1,1,128,512]{2,3,1,0:T(8,128)(2,1)S(1)} %get-tuple-element.110, bf16[1,1,128,512]{2,3,1,0:T(8,128)(2,1)} %get-tuple-element.111, bf16[1,1,128,512]{2,3,1,0:T(8,128)(2,1)} %get-tuple-element.112, bf16[1,1,128,512]{2,3,1,0:T(8,128)(2,1)S(1)} %get-tuple-element.109), kind=kLoop, calls=%fused_computation.26 | loop fusion | flops 786432 | bytes 1048576 | tf_op jit(solution)/shard_map/stack | solution.py:149
  85.7 2.3 %copy.80 = bf16[1,1024,512]{1,2,0:T(8,128)(2,1)} copy(bf16[1,1024,512]{2,1,0:T(8,128)(2,1)} %param.33) | data formatting | bytes 2097152 | tf_op args[14]
  88.0 1.5 %all-to-all-done.1 = f32[4,1,1024]{2,1,0:T(1,128)S(1)} async-done(((f32[4,1,1024]{2,1,0:T(1,128)}), f32[4,1,1024]{2,1,0:T(1,128)S(1)}, u32[]{:S(2)}, u32[]{:S(2)}) %all-to-all-start.1) | async-done | bytes 16416 | tf_op jit(solution)/shard_map/all_to_all | solution.py:152
  89.5 3.6 %all-to-all-start.2 = ((bf16[4,1,128,512]{2,3,1,0:T(8,128)(2,1)}), bf16[4,1,128,512]{2,3,1,0:T(8,128)(2,1)S(1)}, u32[]{:S(2)}, u32[]{:S(2)}) async-start(bf16[4,1,128,512]{2,3,1,0:T(8,128)(2,1)} %pad_maximum_fusion.3), calls=%async_computation.2 | async-start | bytes 1048576 | tf_op jit(solution)/shard_map/all_to_all | solution.py:149
  93.1 0.7 fusion.30
  93.9 1.6 %fusion.20 = f32[8,1,64]{2,1,0:T(1,128)S(1)} fusion(bf16[1024,8,64]{0,2,1:T(8,128)(2,1)} %bitcast.96, bf16[8,1024,1]{1,0,2:T(8,128)(2,1)S(1)} %get-tuple-element.114), kind=kOutput, calls=%fused_computation.44 | convolution fusion | flops 1048576 | bytes 1067008 | tf_op jit(solution)/shard_map/bhl,blhd->bhd/dot_general | solution.py:183
  95.6 0.3 reshape.238
  95.9 0.7 reduce.21
  96.6 0.4 reshape.252
  97.0 0.7 reduce.23
  97.8 0.4 reshape.254
  98.2 0.7 reduce_max.28
  98.9 1.5 %fusion.40 = (f32[128,8]{1,0:T(8,128)}, f32[4,128,8]{2,1,0:T(8,128)S(1)}) fusion(f32[4,128,8]{2,1,0:T(8,128)S(1)} %bitcast.93, f32[4,128,8]{2,1,0:T(8,128)S(1)} %bitcast.92, f32[128,8]{1,0:T(8,128)} %reduce_max.28), kind=kLoop, calls=%fused_computation.78 | loop fusion | flops 11264 | bytes 57344 | tf_op jit(solution)/shard_map/reduce_sum | solution.py:88
  100.5 0.9 copy.74
  101.4 2.0 %all-to-all-done.2 = bf16[4,1,128,512]{2,3,1,0:T(8,128)(2,1)S(1)} async-done(((bf16[4,1,128,512]{2,3,1,0:T(8,128)(2,1)}), bf16[4,1,128,512]{2,3,1,0:T(8,128)(2,1)S(1)}, u32[]{:S(2)}, u32[]{:S(2)}) %all-to-all-start.2) | async-done | bytes 524320 | tf_op jit(solution)/shard_map/all_to_all | solution.py:149
  103.5 0.1 multiply_reduce_fusion
  103.7 2.2 %all_gather.15 = bf16[129,1024]{0,1:T(8,128)(2,1)S(1)} all-gather(bf16[129,512]{0,1:T(8,128)(2,1)S(1)} %pad_maximum_fusion.4), channel_id=1, replica_groups=mesh['dp'=4,'kv'=4,'tp'=2] {'tp'}, dimensions={1}, use_global_device_ids=true | all-gather | bytes 396288 | tf_op jit(solution)/shard_map/all_gather | solution.py:199
  105.9 0.5 convolution_convert_fusion
  106.3 0.7 slice.63
  107.1 0.6 slice.64
  (60 shorter events, 1.6 us)
Async XLA Ops:
  0.6 105.2 %copy-start = (bf16[1024,1024]{1,0:T(8,128)(2,1)S(1)}, bf16[1024,1024]{1,0:T(8,128)(2,1)}, u32[]{:S(2)}) copy-start(bf16[1024,1024]{1,0:T(8,128)(2,1)} %param.27) | copy-start | bytes 6291460
  0.6 3.8 %copy-start.11 = (u32[32]{0:T(128)S(1)}, u32[32]{0:T(128)}, u32[]{:S(2)}) copy-start(u32[32]{0:T(128)} %constant.74) | copy-start | bytes 388
  0.7 19.4 %copy-start.3 = (bf16[128,2048]{1,0:T(8,128)(2,1)S(1)}, bf16[128,2048]{1,0:T(8,128)(2,1)}, u32[]{:S(2)}) copy-start(bf16[128,2048]{1,0:T(8,128)(2,1)} %param.19) | copy-start | bytes 1572868
  0.7 19.4 %copy-start.8 = (bf16[1,2048]{1,0:T(2,128)(2,1)S(1)}, bf16[1,2048]{1,0:T(2,128)(2,1)}, u32[]{:S(2)}) copy-start(bf16[1,2048]{1,0:T(2,128)(2,1)} %param.20) | copy-start | bytes 12292
  0.7 19.4 %copy-start.10 = (f32[2048]{0:T(1024)S(1)}, f32[2048]{0:T(1024)}, u32[]{:S(2)}) copy-start(f32[2048]{0:T(1024)} %param.21) | copy-start | bytes 24580
  0.7 19.2 %copy-start.9 = (f32[16]{0:T(128)S(1)}, f32[16]{0:T(128)}, u32[]{:S(2)}) copy-start(f32[16]{0:T(128)} %param.31) | copy-start | bytes 196
  19.6 2.7 %copy-start.2 = (bf16[512,512]{1,0:T(8,128)(2,1)S(1)}, bf16[512,512]{1,0:T(8,128)(2,1)}, u32[]{:S(2)}) copy-start(bf16[512,512]{1,0:T(8,128)(2,1)} %param.28) | copy-start | bytes 1572868
  23.4 18.7 %copy-start.7 = (f32[8,512]{1,0:T(8,128)S(1)}, f32[8,512]{1,0:T(8,128)}, u32[]{:S(2)}) copy-start(f32[8,512]{1,0:T(8,128)} %param.30) | copy-start | bytes 49156
  25.7 0.7 copy-start.5
  46.1 4.0 %copy-start.1 = (f32[8,512,640]{2,1,0:T(8,128)}, f32[8,512,640]{2,1,0:T(8,128)S(1)}, u32[]{:S(2)}) copy-start(f32[8,512,640]{2,1,0:T(8,128)S(1)} %get-tuple-element.120) | copy-start | bytes 31457284
  46.1 11.0 %copy-start.6 = (f32[1,8,1024]{2,1,0:T(8,128)S(1)}, f32[1,8,1024]{2,1,0:T(8,128)}, u32[]{:S(2)}) copy-start(f32[1,8,1024]{2,1,0:T(8,128)} %param.34) | copy-start | bytes 98308
  52.9 26.1 %all-to-all-start = ((f32[4,1,1024]{2,1,0:T(1,128)}), f32[4,1,1024]{2,1,0:T(1,128)S(1)}, u32[]{:S(2)}, u32[]{:S(2)}) async-start(f32[4,1,1024]{2,1,0:T(1,128)} %reshape.251), calls=%async_computation | async-start | bytes 32768 | tf_op jit(solution)/shard_map/all_to_all | solution.py:153
  63.8 0.7 copy-start.4
  79.0 10.5 %all-to-all-start.1 = ((f32[4,1,1024]{2,1,0:T(1,128)}), f32[4,1,1024]{2,1,0:T(1,128)S(1)}, u32[]{:S(2)}, u32[]{:S(2)}) async-start(f32[4,1,1024]{2,1,0:T(1,128)} %reshape.253), calls=%async_computation.1 | async-start | bytes 32768 | tf_op jit(solution)/shard_map/all_to_all | solution.py:152
  89.5 13.9 %all-to-all-start.2 = ((bf16[4,1,128,512]{2,3,1,0:T(8,128)(2,1)}), bf16[4,1,128,512]{2,3,1,0:T(8,128)(2,1)S(1)}, u32[]{:S(2)}, u32[]{:S(2)}) async-start(bf16[4,1,128,512]{2,3,1,0:T(8,128)(2,1)} %pad_maximum_fusion.3), calls=%async_computation.2 | async-start | bytes 1048576 | tf_op jit(solution)/shard_map/all_to_all | solution.py:149
